TPU v7x, 1024 devices: a whole 4x8x16 slice. The times are simulated.
1024 devices in a mesh: ep: 32 (over z, core), tp: 32 (over y, x).
Axes of the slice: x: 4, y: 8, z: 16, core: 2. Of those that a mesh axis runs over, the one named last changes fastest.
Arguments:
- tokens: bfloat16 [256, 2048], P('ep'), may hold values from -6 to 6
- attn_gain: float32 [2048], replicated, may hold values from 0.1 to 1.9
- query_weight: bfloat16 [2048, 4096], P('ep', 'tp'), may hold values from -0.125 to 0.125
- key_weight: bfloat16 [2048, 4096], P('ep', 'tp'), may hold values from -0.125 to 0.125
- value_weight: bfloat16 [2048, 4096], P('ep', 'tp'), may hold values from -0.125 to 0.125
- query_gain: float32 [128], replicated, may hold values from 0.1 to 1.9
- stick_bias: float32 [32], P('tp'), may hold values from -7 to -2.5
- key_cache: bfloat16 [256, 32, 512, 128], P('ep', 'tp'), may hold values from -6 to 6
- value_cache: bfloat16 [256, 32, 512, 128], P('ep', 'tp'), may hold values from -6 to 6
- lengths: int32 [256], P('ep'), may hold values from 64 to 512, as said below
- out_weight: bfloat16 [4096, 2048], P('tp'), may hold values from -0.375 to 0.375
- mix_gain: float32 [2048], replicated, may hold values from 0.1 to 1.9
- route_ids: int32 [256, 2], P('ep'), may hold values from 0 to 31, all different within a row; in each aligned block of 8 rows (0 to 7, 8 to 15, ...) at most 2 rows name the same one
- route_weights: float32 [256, 2], P('ep'), may hold values from 0.2 to 1
- expert_gate: bfloat16 [32, 2048, 2560], P('ep', None, 'tp'), may hold values from -0.125 to 0.125
- expert_up: bfloat16 [32, 2048, 2560], P('ep', None, 'tp'), may hold values from -0.125 to 0.125
- expert_down: bfloat16 [32, 2560, 2048], P('ep', 'tp'), may hold values from -0.21875 to 0.21875
- side_gate: bfloat16 [2048, 1024], P(None, 'tp'), may hold values from -0.125 to 0.125
- side_up: bfloat16 [2048, 1024], P(None, 'tp'), may hold values from -0.125 to 0.125
- side_down: bfloat16 [1024, 2048], P('tp'), may hold values from -0.375 to 0.375
- branch_gate: float32 [2048], replicated, may hold values from -0.125 to 0.125
Outputs:
- mixed: bfloat16 [256, 2048], P('ep', 'tp')
- new_keys: bfloat16 [256, 4096], P('ep', 'tp')
- new_values: bfloat16 [256, 4096], P('ep', 'tp')
Inputs may be any that keep to these rules, and one draw needn't show every extreme that they name: `lengths`: at least an eighth of 512; the first sequence has 512. `route_ids`: each token names 2 different experts. In the rows of one device no expert is named by more than 2 rows, a bound that some block reaches of some device.
All inputs are finite; a program needn't handle non-finite values.
Results may differ from a plain program's by a relative error of at most 0.018.
Values may be sent and summed in bfloat16 or wider, within the bound.
A program may use at most 32 MiB of HBM per device.

v0:
```python
import jax
import jax.numpy as jnp
from jax import lax
from jax.sharding import PartitionSpec as P

DH = 128


epsilon = 1e-06


def split_up(value, dim, size):
    lengths = value.shape
    parts = value.reshape(*lengths[:dim], size, lengths[dim] // size, *lengths[dim + 1 :])
    return jnp.moveaxis(parts, dim, 0)


def sum_at_owner(value, axis, dim):
    parts = split_up(value, dim, lax.axis_size(axis))
    arrived = lax.all_to_all(parts, axis, split_axis=0, concat_axis=0, tiled=True)
    return arrived.sum(axis=0)


def copy_for_each(value, axis):
    copies = jnp.broadcast_to(value, (lax.axis_size(axis), *value.shape))
    return lax.all_to_all(copies, axis, split_axis=0, concat_axis=0, tiled=True)


def taken_together(value, axis):
    everything = copy_for_each(value, axis)
    return jnp.sum(everything.astype(jnp.float32), axis=0)


def sent_and_summed(value, axis, dim):
    size = lax.axis_size(axis)
    parts = lax.all_to_all(split_up(value, dim, size), axis, 0, 0, tiled=True)
    return jnp.sum(parts.astype(jnp.float32), axis=0)


def side_by_side(arrays, axis, dim, along):
    ends, at = ([], 0)
    for a in arrays[:-1]:
        at += a.shape[along]
        ends.append(at)
    both = jnp.concatenate(arrays, axis=along)
    return tuple(jnp.split(sent_and_summed(both, axis, dim), ends, axis=along))


def rms_scale(values, scale_gain):
    mean_square = jnp.mean(values * values, axis=-1, keepdims=True)
    return values * lax.rsqrt(mean_square + epsilon) * scale_gain


def body(
    tokens,
    attn_gain,
    query_weight,
    key_weight,
    value_weight,
    query_gain,
    stick_bias,
    key_cache,
    value_cache,
    lengths,
    out_weight,
    mix_gain,
    route_ids,
    route_weights,
    expert_gate,
    expert_up,
    expert_down,
    side_gate,
    side_up,
    side_down,
    branch_gate,
):
    seq_count, model_width = tokens.shape
    head_cols = query_weight.shape[1]
    heads_local = key_cache.shape[1]
    cache_slots = key_cache.shape[2]
    stream = tokens.astype(jnp.float32)
    normed = rms_scale(stream, attn_gain).astype(jnp.bfloat16)
    stacked = jnp.concatenate([query_weight, key_weight, value_weight], axis=1)
    columns = lax.all_to_all(normed, "ep", split_axis=1, concat_axis=0, tiled=True)
    picked = columns
    projected = sum_at_owner(jnp.dot(picked, stacked, preferred_element_type=jnp.float32), "ep", 0)
    query_rows = projected[:, :head_cols].astype(jnp.bfloat16)
    fresh_keys = projected[:, head_cols : 2 * head_cols].astype(jnp.bfloat16)
    new_values = projected[:, 2 * head_cols :].astype(jnp.bfloat16)
    new_keys = rms_scale(fresh_keys.astype(jnp.float32).reshape(seq_count, heads_local, DH), 1.0)
    new_keys = new_keys.astype(jnp.bfloat16).reshape(seq_count, head_cols)
    query_heads = rms_scale(
        query_rows.astype(jnp.float32).reshape(seq_count, heads_local, DH), query_gain
    )
    query_heads = query_heads.astype(jnp.bfloat16)
    scores = jnp.einsum("shd,shld->shl", query_heads, key_cache, preferred_element_type=jnp.float32)
    scores = scores * DH ** (-0.5) + stick_bias[None, :, None]
    positions = jnp.arange(cache_slots, dtype=jnp.int32)
    visible = positions[None, None, :] < lengths[:, None, None]
    log_rest = jnp.where(visible, jax.nn.log_sigmoid(-scores), 0.0)
    log_between = lax.cumsum(log_rest, axis=2, reverse=True) - log_rest
    stick = jnp.where(visible, jnp.exp(jax.nn.log_sigmoid(scores) + log_between), 0.0).astype(
        jnp.bfloat16
    )
    attended = jnp.einsum("shl,shld->shd", stick, value_cache, preferred_element_type=jnp.float32)
    attended = attended.astype(jnp.bfloat16).reshape(seq_count, head_cols)
    attn_proj = taken_together(
        jnp.dot(attended, out_weight, preferred_element_type=jnp.float32).astype(jnp.bfloat16), "tp"
    ).astype(jnp.float32)
    middle = (stream + attn_proj).astype(jnp.bfloat16)
    normed_mix = rms_scale(middle.astype(jnp.float32), mix_gain).astype(jnp.bfloat16)
    side_gate_pre = jnp.dot(normed_mix, side_gate, preferred_element_type=jnp.float32)
    side_up_pre = jnp.dot(normed_mix, side_up, preferred_element_type=jnp.float32)
    side_hidden = (jax.nn.silu(side_gate_pre) * side_up_pre).astype(jnp.bfloat16)
    side_term = jnp.dot(side_hidden, side_down, preferred_element_type=jnp.float32)
    switch = jax.nn.sigmoid(
        jnp.sum(normed_mix.astype(jnp.float32) * branch_gate, axis=1, keepdims=True)
    )
    experts = lax.axis_size("ep")
    top_count = route_ids.shape[1]
    capacity = max(2, 2 * top_count * seq_count // experts)
    flat_ids = route_ids.reshape(-1)
    onehot = (flat_ids[:, None] == jnp.arange(experts, dtype=jnp.int32)[None, :]).astype(jnp.int32)
    before = jnp.cumsum(onehot, axis=0) - onehot
    slot_index = jnp.sum(before * onehot, axis=1)
    target = flat_ids * capacity + slot_index
    route_map = (
        target[:, None] == jnp.arange(experts * capacity, dtype=jnp.int32)[None, :]
    ).astype(jnp.bfloat16)
    dispatch = jnp.sum(route_map.reshape(seq_count, top_count, experts * capacity), axis=1).T
    outbox = jnp.dot(dispatch, normed_mix, preferred_element_type=jnp.float32).astype(jnp.bfloat16)
    outbox = outbox.reshape(experts, capacity, model_width)
    col_width = model_width // lax.axis_size("tp")
    col_offset = lax.axis_index("tp") * col_width
    arrived = lax.all_to_all(outbox, "ep", split_axis=0, concat_axis=0, tiled=True)
    slot_rows = arrived.reshape(experts * capacity, model_width)
    gate_pre = jnp.dot(slot_rows, expert_gate[0], preferred_element_type=jnp.float32)
    up_pre = jnp.dot(slot_rows, expert_up[0], preferred_element_type=jnp.float32)
    hidden = (jax.nn.silu(gate_pre) * up_pre).astype(jnp.bfloat16)
    expert_term = jnp.dot(hidden, expert_down[0], preferred_element_type=jnp.float32)
    expert_part, side_part = side_by_side(
        (expert_term.astype(jnp.bfloat16), side_term.astype(jnp.bfloat16)), "tp", 1, 0
    )
    returned = lax.all_to_all(
        expert_part.astype(jnp.bfloat16).reshape(experts, capacity, col_width),
        "ep",
        split_axis=0,
        concat_axis=0,
        tiled=True,
    )
    picked = jnp.dot(
        route_map,
        returned.reshape(experts * capacity, col_width),
        preferred_element_type=jnp.float32,
    )
    routed = jnp.sum(
        route_weights[:, :, None] * picked.reshape(seq_count, top_count, col_width), axis=1
    )
    middle_cols = lax.dynamic_slice_in_dim(middle, col_offset, col_width, 1).astype(jnp.float32)
    mixed = (middle_cols + routed + switch * side_part).astype(jnp.bfloat16)
    return (mixed, new_keys, new_values)


def solution(mesh):
    in_specs = (
        P("ep", None),
        P(),
        P("ep", "tp"),
        P("ep", "tp"),
        P("ep", "tp"),
        P(),
        P("tp"),
        P("ep", "tp", None, None),
        P("ep", "tp", None, None),
        P("ep"),
        P("tp", None),
        P(),
        P("ep", None),
        P("ep", None),
        P("ep", None, "tp"),
        P("ep", None, "tp"),
        P("ep", "tp", None),
        P(None, "tp"),
        P(None, "tp"),
        P("tp", None),
        P(),
    )
    out_specs = (P("ep", "tp"), P("ep", "tp"), P("ep", "tp"))
    return jax.shard_map(body, mesh=mesh, in_specs=in_specs, out_specs=out_specs, check_vma=False)
```

profile of v0, /device:TPU:1, one launch (start us, length us, event | category | flops | bytes accessed | tf_op | source)
XLA Modules:
  0.0 187.5 jit_solution(6174132449406601958)
XLA Ops:
  0.6 0.0 copy-start
  0.6 1.0 fusion.15
  1.6 0.8 fusion.17
  2.5 0.1 all_to_all.27
  2.6 0.0 copy-start.13
  2.7 0.1 reshape.229
  2.8 32.3 %all_to_all.41 = bf16[32,2,256]{2,1,0:T(2,128)(2,1)S(1)} all-to-all(bf16[32,2,256]{2,1,0:T(2,128)(2,1)S(1)} %reshape.229), channel_id=1, replica_groups=mesh['ep'=32,'tp'=32] {'ep'}, dimensions={0} | all-to-all | bytes 65536 | tf_op jit(solution)/shard_map/all_to_all | solution.py:84
  35.0 0.1 reshape.230
  35.1 1.7 fusion.19
  36.8 4.8 %all-to-all-start.1 = ((f32[32,8,384]{2,1,0:T(8,128)}), f32[32,8,384]{2,1,0:T(8,128)S(1)}, u32[]{:S(2)}, u32[]{:S(2)}) async-start(f32[32,8,384]{2,1,0:T(8,128)} %fusion.19), calls=%async_computation.1 | async-start | bytes 786432 | tf_op jit(solution)/shard_map/all_to_all | solution.py:20
  42.3 27.2 %all-to-all-done.1 = f32[32,8,384]{2,1,0:T(8,128)S(1)} async-done(((f32[32,8,384]{2,1,0:T(8,128)}), f32[32,8,384]{2,1,0:T(8,128)S(1)}, u32[]{:S(2)}, u32[]{:S(2)}) %all-to-all-start.1) | async-done | bytes 393248 | tf_op jit(solution)/shard_map/all_to_all | solution.py:20
  69.6 0.1 fusion.50
  69.7 0.7 fusion.51
  70.4 0.0 copy-done
  70.4 0.4 fusion.5
  70.8 0.1 fusion.41
  70.8 5.0 %reduce-window.6 = f32[8,1,4,128]{3,0,1,2:T(8,128)S(1)} reduce-window(f32[8,1,4,128]{3,0,1,2:T(8,128)S(1)} %fusion.41, f32[]{:T(128)} %constant.17.clone.1), window={size=1x1x1x128 pad=0_0x0_0x0_0x0_127}, to_apply=%region_3.0 | reduce-window | flops 520192 | bytes 32772 | tf_op jit(solution)/shard_map/reduce-window
  75.8 0.1 slice_reduce_fusion
  75.9 0.1 fusion.46
  76.0 0.2 fusion.3
  76.3 0.0 copy-done.2
  76.3 0.2 convolution_convert_fusion.3
  76.5 1.1 broadcast_in_dim.4
  77.6 9.8 %all-to-all-start.2 = ((bf16[32,8,2048]{2,1,0:T(8,128)(2,1)}), bf16[32,8,2048]{2,1,0:T(8,128)(2,1)S(1)}, u32[]{:S(2)}, u32[]{:S(2)}) async-start(bf16[32,8,2048]{2,1,0:T(8,128)(2,1)} %broadcast_in_dim.4), calls=%async_computation.2 | async-start | bytes 2097152 | tf_op jit(solution)/shard_map/all_to_all | solution.py:26
  87.4 0.0 copy-start.6
  87.4 0.0 copy-start.9
  87.4 0.1 copy.65
  87.5 0.1 eq.51
  87.6 0.1 fusion.42
  87.7 0.2 select_reduce_fusion
  87.9 0.1 reduce_sum.109
  88.0 0.1 copy.67
  88.1 0.1 fusion.52
  88.1 25.4 %all-to-all-done.2 = bf16[32,8,2048]{2,1,0:T(8,128)(2,1)S(1)} async-done(((bf16[32,8,2048]{2,1,0:T(8,128)(2,1)}), bf16[32,8,2048]{2,1,0:T(8,128)(2,1)S(1)}, u32[]{:S(2)}, u32[]{:S(2)}) %all-to-all-start.2) | async-done | bytes 1048608 | tf_op jit(solution)/shard_map/all_to_all | solution.py:26
  113.5 0.2 convert_reduce_fusion
  113.7 0.0 copy-start.7
  113.7 0.0 copy-start.8
  113.7 0.1 fusion.12
  113.9 0.3 convolution_convert_fusion.1
  114.1 0.0 copy-start.3
  114.2 0.9 reshape.217
  115.0 6.5 %all-to-all-start.3 = ((bf16[32,2,2048]{2,1,0:T(2,128)(2,1)}), bf16[32,2,2048]{2,1,0:T(2,128)(2,1)S(1)}, u32[]{:S(2)}, u32[]{:S(2)}) async-start(bf16[32,2,2048]{2,1,0:T(2,128)(2,1)} %reshape.217), calls=%async_computation.3 | async-start | bytes 524288 | tf_op jit(solution)/shard_map/all_to_all | solution.py:135
  121.6 0.2 fusion.68
  121.8 0.0 copy-done.7
  121.8 0.4 convolution_convert_fusion.2
  122.2 21.0 %all-to-all-done.3 = bf16[32,2,2048]{2,1,0:T(2,128)(2,1)S(1)} async-done(((bf16[32,2,2048]{2,1,0:T(2,128)(2,1)}), bf16[32,2,2048]{2,1,0:T(2,128)(2,1)S(1)}, u32[]{:S(2)}, u32[]{:S(2)}) %all-to-all-start.3) | async-done | bytes 262176 | tf_op jit(solution)/shard_map/all_to_all | solution.py:135
  143.2 0.1 reshape.218
  143.3 0.2 fusion.10
  143.6 0.5 convolution_convert_fusion
  144.2 0.6 reshape.219
  144.8 0.0 copy-start.10
  144.8 1.4 copy.69
  146.2 5.4 %all-to-all-start.4 = ((bf16[32,72,64]{1,2,0:T(8,128)(2,1)}), bf16[32,72,64]{1,2,0:T(8,128)(2,1)S(1)}, u32[]{:S(2)}, u32[]{:S(2)}) async-start(bf16[32,72,64]{1,2,0:T(8,128)(2,1)} %copy.69), calls=%async_computation.4 | async-start | bytes 1048576 | tf_op jit(solution)/shard_map/all_to_all | solution.py:36
  151.7 0.6 slice.26
  152.2 0.2 multiply_reduce_fusion
  152.4 14.5 %all-to-all-done.4 = bf16[32,72,64]{1,2,0:T(8,128)(2,1)S(1)} async-done(((bf16[32,72,64]{1,2,0:T(8,128)(2,1)}), bf16[32,72,64]{1,2,0:T(8,128)(2,1)S(1)}, u32[]{:S(2)}, u32[]{:S(2)}) %all-to-all-start.4) | async-done | bytes 294944 | tf_op jit(solution)/shard_map/all_to_all | solution.py:36
  167.0 0.1 convert_reduce_fusion.1
  167.1 0.7 copy.70
  167.8 7.0 %all-to-all-start.5 = ((bf16[32,2,64]{2,1,0:T(2,128)(2,1)}), bf16[32,2,64]{2,1,0:T(2,128)(2,1)S(1)}, u32[]{:S(2)}, u32[]{:S(2)}) async-start(bf16[32,2,64]{2,1,0:T(2,128)(2,1)} %bitcast.19), calls=%async_computation.5 | async-start | bytes 32768 | tf_op jit(solution)/shard_map/all_to_all | solution.py:144
  174.8 0.1 split.10
  174.9 0.1 copy.76
  174.9 11.8 %all-to-all-done.5 = bf16[32,2,64]{2,1,0:T(2,128)(2,1)S(1)} async-done(((bf16[32,2,64]{2,1,0:T(2,128)(2,1)}), bf16[32,2,64]{2,1,0:T(2,128)(2,1)S(1)}, u32[]{:S(2)}, u32[]{:S(2)}) %all-to-all-start.5) | async-done | bytes 8224 | tf_op jit(solution)/shard_map/all_to_all | solution.py:144
  186.7 0.2 fusion.1
  186.9 0.7 add_convert_fusion
  (33 shorter events, 0.3 us)
Async XLA Ops:
  0.6 69.7 %copy-start = (bf16[8,1,512,128]{3,2,1,0:T(8,128)(2,1)S(1)}, bf16[8,1,512,128]{3,2,1,0:T(8,128)(2,1)}, u32[]{:S(2)}) copy-start(bf16[8,1,512,128]{3,2,1,0:T(8,128)(2,1)} %param.28) | copy-start | bytes 3145732
  2.6 67.1 %copy-start.13 = (f32[128]{0:T(128)S(1)}, f32[128]{0:T(128)}, u32[]{:S(2)}) copy-start(f32[128]{0:T(128)} %param.26) | copy-start | bytes 1540
  36.8 33.9 %copy-start.11 = (s32[8]{0:T(128)S(1)}, s32[8]{0:T(128)}, u32[]{:S(2)}) copy-start(s32[8]{0:T(128)} %param.30) | copy-start | bytes 100
  36.8 39.2 %copy-start.1 = (bf16[8,1,512,128]{3,2,1,0:T(8,128)(2,1)S(1)}, bf16[8,1,512,128]{3,2,1,0:T(8,128)(2,1)}, u32[]{:S(2)}) copy-start(bf16[8,1,512,128]{3,2,1,0:T(8,128)(2,1)} %param.29) | copy-start | bytes 3145732
  36.8 32.7 %all-to-all-start.1 = ((f32[32,8,384]{2,1,0:T(8,128)}), f32[32,8,384]{2,1,0:T(8,128)S(1)}, u32[]{:S(2)}, u32[]{:S(2)}) async-start(f32[32,8,384]{2,1,0:T(8,128)} %fusion.19), calls=%async_computation.1 | async-start | bytes 786432 | tf_op jit(solution)/shard_map/all_to_all | solution.py:20
  70.4 5.9 %copy-start.2 = (bf16[128,2048]{1,0:T(8,128)(2,1)S(1)}, bf16[128,2048]{1,0:T(8,128)(2,1)}, u32[]{:S(2)}) copy-start(bf16[128,2048]{1,0:T(8,128)(2,1)} %param.31) | copy-start | bytes 1572868
  77.6 9.8 %copy-start.12 = (s32[8,2]{0,1:T(2,128)S(1)}, s32[8,2]{0,1:T(2,128)}, u32[]{:S(2)}) copy-start(s32[8,2]{0,1:T(2,128)} %param.33) | copy-start | bytes 196
  77.6 35.9 %all-to-all-start.2 = ((bf16[32,8,2048]{2,1,0:T(8,128)(2,1)}), bf16[32,8,2048]{2,1,0:T(8,128)(2,1)S(1)}, u32[]{:S(2)}, u32[]{:S(2)}) async-start(bf16[32,8,2048]{2,1,0:T(8,128)(2,1)} %broadcast_in_dim.4), calls=%async_computation.2 | async-start | bytes 2097152 | tf_op jit(solution)/shard_map/all_to_all | solution.py:26
  87.4 26.3 %copy-start.6 = (bf16[8,2048]{1,0:T(8,128)(2,1)S(1)}, bf16[8,2048]{1,0:T(8,128)(2,1)}, u32[]{:S(2)}) copy-start(bf16[8,2048]{1,0:T(8,128)(2,1)} %param.21) | copy-start | bytes 98308
  87.4 26.4 %copy-start.9 = (f32[2048]{0:T(1024)S(1)}, f32[2048]{0:T(1024)}, u32[]{:S(2)}) copy-start(f32[2048]{0:T(1024)} %param.32) | copy-start | bytes 24580
  88.1 33.4 %copy-start.14 = (bf16[2048,32]{0,1:T(8,128)(2,1)S(1)}, bf16[2048,32]{0,1:T(8,128)(2,1)}, u32[]{:S(2)}) copy-start(bf16[2048,32]{0,1:T(8,128)(2,1)} %param.38) | copy-start | bytes 393220
  113.7 8.1 %copy-start.7 = (bf16[32,2048]{1,0:T(8,128)(2,1)S(1)}, bf16[32,2048]{1,0:T(8,128)(2,1)}, u32[]{:S(2)}) copy-start(bf16[32,2048]{1,0:T(8,128)(2,1)} %param.40) | copy-start | bytes 393220
  113.7 8.1 %copy-start.8 = (bf16[2048,32]{0,1:T(8,128)(2,1)S(1)}, bf16[2048,32]{0,1:T(8,128)(2,1)}, u32[]{:S(2)}) copy-start(bf16[2048,32]{0,1:T(8,128)(2,1)} %param.39) | copy-start | bytes 393220
  114.1 29.2 %copy-start.3 = (bf16[1,2048,80]{1,2,0:T(8,128)(2,1)S(1)}, bf16[1,2048,80]{1,2,0:T(8,128)(2,1)}, u32[]{:S(2)}) copy-start(bf16[1,2048,80]{1,2,0:T(8,128)(2,1)} %param.35) | copy-start | bytes 983044
  115.0 28.5 %copy-start.4 = (bf16[1,80,2048]{2,1,0:T(8,128)(2,1)S(1)}, bf16[1,80,2048]{2,1,0:T(8,128)(2,1)}, u32[]{:S(2)}) copy-start(bf16[1,80,2048]{2,1,0:T(8,128)(2,1)} %param.37) | copy-start | bytes 983044
  115.0 28.6 %copy-start.5 = (bf16[1,2048,80]{1,2,0:T(8,128)(2,1)S(1)}, bf16[1,2048,80]{1,2,0:T(8,128)(2,1)}, u32[]{:S(2)}) copy-start(bf16[1,2048,80]{1,2,0:T(8,128)(2,1)} %param.36) | copy-start | bytes 983044
  115.0 28.2 %all-to-all-start.3 = ((bf16[32,2,2048]{2,1,0:T(2,128)(2,1)}), bf16[32,2,2048]{2,1,0:T(2,128)(2,1)S(1)}, u32[]{:S(2)}, u32[]{:S(2)}) async-start(bf16[32,2,2048]{2,1,0:T(2,128)(2,1)} %reshape.217), calls=%async_computation.3 | async-start | bytes 524288 | tf_op jit(solution)/shard_map/all_to_all | solution.py:135
  144.8 7.5 %copy-start.10 = (f32[2048]{0:T(1024)S(1)}, f32[2048]{0:T(1024)}, u32[]{:S(2)}) copy-start(f32[2048]{0:T(1024)} %param.41) | copy-start | bytes 24580
  146.2 40.5 %copy-start.15 = (f32[8,2]{0,1:T(2,128)S(1)}, f32[8,2]{0,1:T(2,128)}, u32[]{:S(2)}) copy-start(f32[8,2]{0,1:T(2,128)} %param.34) | copy-start | bytes 196
  146.2 20.7 %all-to-all-start.4 = ((bf16[32,72,64]{1,2,0:T(8,128)(2,1)}), bf16[32,72,64]{1,2,0:T(8,128)(2,1)S(1)}, u32[]{:S(2)}, u32[]{:S(2)}) async-start(bf16[32,72,64]{1,2,0:T(8,128)(2,1)} %copy.69), calls=%async_computation.4 | async-start | bytes 1048576 | tf_op jit(solution)/shard_map/all_to_all | solution.py:36
  167.8 18.9 %all-to-all-start.5 = ((bf16[32,2,64]{2,1,0:T(2,128)(2,1)}), bf16[32,2,64]{2,1,0:T(2,128)(2,1)S(1)}, u32[]{:S(2)}, u32[]{:S(2)}) async-start(bf16[32,2,64]{2,1,0:T(2,128)(2,1)} %bitcast.19), calls=%async_computation.5 | async-start | bytes 32768 | tf_op jit(solution)/shard_map/all_to_all | solution.py:144
where the time goes:
time: 188 us
  waiting for transfers between devices  99.9 us (53%)
  starting transfers between devices  33.6 us (18%)
  blocking collectives  32.3 us (17%)
  other arithmetic  9.51 us (5%)
  local copies, waits for them, and re-layouts  6.44 us (3%)
  matrix products  4.27 us (2%)
    all_to_all x1, blocking collectives, body(): lax.all_to_all(normed, 'ep', split_axis=1, concat_axis=0, tiled=True)  32.3 us
    all_to_all x1, waiting for transfers between devices, sum_at_owner(): lax.all_to_all(parts, axis, split_axis=0, concat_axis=0, tiled=True)  27.2 us
    all_to_all x1, waiting for transfers between devices, copy_for_each(): return lax.all_to_all(copies, axis, split_axis=0, concat_axis=0, tiled=True)  25.4 us
    all_to_all x1, waiting for transfers between devices, body(): lax.all_to_all(outbox, 'ep', split_axis=0, concat_axis=0, tiled=True)  21 us
    all_to_all x1, waiting for transfers between devices, sent_and_summed(): parts = lax.all_to_all(split_up(value, dim, size), axis, 0, 0, tiled=True)  14.5 us
    all_to_all x1, waiting for transfers between devices, body(): lax.all_to_all(expert_part.astype(jnp.bfloat16).reshape(experts, capacity...  11.8 us
    all_to_all x1, starting transfers between devices, copy_for_each(): return lax.all_to_all(copies, axis, split_axis=0, concat_axis=0, tiled=True)  9.8 us
    all_to_all x1, starting transfers between devices, body(): lax.all_to_all(expert_part.astype(jnp.bfloat16).reshape(experts, capacity...  7 us
  transfers between devices with their start and end apart: 5, of which 5 were waited for; matrix products, arithmetic and copies ran while one was open for 1% of the time, Pallas kernels for 0%

commit v1 on v0

v1 whole, which is shorter than its diff:
```python
import functools

import jax
import jax.numpy as jnp
from jax import lax
from jax.experimental import pallas as pl
from jax.experimental.pallas import tpu as pltpu
from jax.sharding import PartitionSpec as P

DH = 128
XN = 4
EPS = 1e-06
F32 = jnp.float32
BF16 = jnp.bfloat16
MESH = pl.DeviceIdType.MESH


def far_first(i, n):
    half = (i + 1) // 2
    return n // 2 + half * (2 * lax.rem(i + 1, 2) - 1)


def log_sigmoids(x):
    t = jnp.log1p(jnp.exp(-jnp.abs(x)))
    return jnp.minimum(x, 0.0) - t, jnp.minimum(-x, 0.0) - t


def kernel(
    ep_n,
    tp_n,
    tokens,
    attn_gain,
    wq,
    wk,
    wv,
    qgain,
    bias,
    kcache,
    vcache,
    lengths,
    oweight,
    mix_gain,
    rids,
    rweights,
    egate,
    eup,
    edown,
    sgate,
    sup,
    sdown,
    bgate,
    mixed_out,
    keys_out,
    values_out,
    tok,
    again,
    mgain,
    qg,
    bg,
    wpad,
    kb,
    vb,
    ow,
    eg,
    eu,
    ed,
    sg,
    su,
    sd,
    tri,
    tiles,
    nsend,
    nrecv,
    qsend,
    qrecv,
    kvsend,
    kvrecv,
    asend,
    arecv,
    mid,
    nmix,
    xo,
    obox,
    ibox,
    xt,
    xg,
    xn,
    ssend,
    srecv,
    esend,
    erecv,
    rsend,
    rrecv,
    ld,
    snd,
    rcv,
):
    me_e = lax.axis_index("ep")
    me_t = lax.axis_index("tp")
    core = lax.rem(me_e, 2)
    yn = tp_n // XN
    my_y = me_t // XN
    my_x = lax.rem(me_t, XN)
    my_k = me_t // 2
    side = lax.rem(me_t, 2)
    kt = tp_n // 2
    seqs, width = tok.shape
    slots = kb.shape[1]

    def ep_peer(i):
        return lax.rem(me_e + far_first(i, ep_n), ep_n)

    def tp_peer(i):
        dy = far_first(i // XN, yn)
        dx = far_first(lax.rem(i, XN), XN)
        return lax.rem(my_y + dy, yn) * XN + lax.rem(my_x + dx, XN)

    barrier = pltpu.get_barrier_semaphore()

    def greet_ep(i, c):
        pl.semaphore_signal(barrier, inc=1, device_id={"ep": ep_peer(i)}, device_id_type=MESH)
        return c

    def greet_tp(i, c):
        pl.semaphore_signal(barrier, inc=1, device_id={"tp": tp_peer(i)}, device_id_type=MESH)
        return c

    lax.fori_loop(0, ep_n - 1, greet_ep, 0)
    lax.fori_loop(0, tp_n - 1, greet_tp, 0)

    rows_w = wq.shape[0]
    at_w = pl.ds(pl.multiple_of(core * rows_w, rows_w), rows_w)
    loads = [
        (tokens, tok),
        (attn_gain, again),
        (wq, wpad.at[at_w, pl.ds(0, DH)]),
        (wk, wpad.at[at_w, pl.ds(DH, DH)]),
        (wv, wpad.at[at_w, pl.ds(2 * DH, DH)]),
        (qgain, qg),
        (kcache.at[:, 0], kb),
        (vcache.at[:, 0], vb),
        (oweight, ow),
        (mix_gain, mgain),
        (bgate, bg),
        (sgate, sg),
        (sup, su),
        (sdown, sd),
        (egate.at[0], eg),
        (eup.at[0], eu),
        (edown.at[0], ed),
    ]
    copies = [pltpu.make_async_copy(a, b, ld.at[i]) for i, (a, b) in enumerate(loads)]
    for c in copies:
        c.start()

    other = pl.ds(pl.multiple_of((1 - core) * rows_w, rows_w), rows_w)
    wpad[other, :] = jnp.zeros((rows_w, 3 * DH), BF16)
    r_i = lax.broadcasted_iota(jnp.int32, (slots, slots), 0)
    c_i = lax.broadcasted_iota(jnp.int32, (slots, slots), 1)
    tri[...] = jnp.where(r_i > c_i, 1.0, 0.0).astype(BF16)

    ids = [rids[b, k] for b in range(seqs) for k in range(2)]
    places = []
    for i in range(2 * seqs):
        n = jnp.int32(0)
        for j in range(i):
            if j // 2 != i // 2:
                n = n + jnp.where(ids[j] == ids[i], 1, 0)
        places.append(n)

    copies[0].wait()
    copies[1].wait()
    stream = tok[...].astype(F32)
    ms = jnp.mean(stream * stream, axis=-1, keepdims=True)
    normed = (stream * lax.rsqrt(ms + EPS) * again[...]).astype(BF16)
    for k in range(kt):
        tiles[k] = stream[:, k * 128 : (k + 1) * 128]
        nsend[k] = normed[:, k * 128 : (k + 1) * 128]
    nrecv[me_e] = nsend[me_e // 2]

    pl.semaphore_wait(barrier, ep_n + tp_n - 2)

    def put_ep(p, src_of, dst):
        def one(i, c):
            f = ep_peer(i)
            pltpu.make_async_remote_copy(
                src_ref=src_of(f),
                dst_ref=dst.at[me_e],
                send_sem=snd.at[p],
                recv_sem=rcv.at[p],
                device_id={"ep": f},
                device_id_type=MESH,
            ).start()
            return c

        lax.fori_loop(0, ep_n - 1, one, 0)

    def put_tp(p, src_of, dst):
        def one(i, c):
            f = tp_peer(i)
            pltpu.make_async_remote_copy(
                src_ref=src_of(f),
                dst_ref=dst.at[me_t],
                send_sem=snd.at[p],
                recv_sem=rcv.at[p],
                device_id={"tp": f},
                device_id_type=MESH,
            ).start()
            return c

        lax.fori_loop(0, tp_n - 1, one, 0)

    def put_tiles(p, buf):
        def one(i, c):
            q = lax.rem(i + 1, 2)
            y = lax.rem(my_y + far_first(i // 2, yn), yn)
            f = y * XN + q * (XN - 1 - my_x) + (1 - q) * my_x
            pltpu.make_async_remote_copy(
                src_ref=buf.at[my_k],
                dst_ref=buf.at[my_k],
                send_sem=snd.at[p],
                recv_sem=rcv.at[p],
                device_id={"tp": f},
                device_id_type=MESH,
            ).start()
            return c

        lax.fori_loop(0, 2 * yn - 1, one, 0)

    def arrived(p, buf, n):
        part = buf.at[pl.ds(0, n)]
        pltpu.make_async_copy(part, part, rcv.at[p]).wait()

    def sent(p, buf, n):
        part = buf.at[pl.ds(0, n)]
        pltpu.make_async_copy(part, part, snd.at[p]).wait()

    put_ep(0, lambda f: nsend.at[f // 2], nrecv)
    for i in (2, 3, 4, 5):
        copies[i].wait()
    arrived(0, nrecv, ep_n - 1)
    picked = nrecv[...].astype(F32).reshape(ep_n * seqs, 128).astype(BF16)
    part = jnp.dot(picked, wpad[:, :DH], preferred_element_type=F32)
    for f in range(ep_n):
        qsend[f] = part[f * seqs : (f + 1) * seqs].astype(BF16)
    put_ep(1, lambda f: qsend.at[f], qrecv)
    qrecv[me_e] = qsend[me_e]
    part = jnp.dot(picked, wpad[:, DH:], preferred_element_type=F32)
    for f in range(ep_n):
        kvsend[f, 0] = part[f * seqs : (f + 1) * seqs, :DH].astype(BF16)
        kvsend[f, 1] = part[f * seqs : (f + 1) * seqs, DH:].astype(BF16)
    put_ep(2, lambda f: kvsend.at[f], kvrecv)
    kvrecv[me_e] = kvsend[me_e]

    row = lax.broadcasted_iota(jnp.int32, (seqs, slots), 0)
    pos = lax.broadcasted_iota(jnp.int32, (seqs, slots), 1)
    lens = jnp.zeros((seqs, slots), jnp.int32)
    for b in range(seqs):
        lens = jnp.where(row == b, lengths[b], lens)
    visible = pos < lens
    copies[6].wait()
    copies[7].wait()
    copies[8].wait()
    arrived(1, qrecv, ep_n - 1)
    q = jnp.sum(qrecv[...].astype(F32), axis=0).astype(BF16).astype(F32)
    ms = jnp.mean(q * q, axis=-1, keepdims=True)
    q = (q * lax.rsqrt(ms + EPS) * qg[...]).astype(BF16)
    scores = jnp.zeros((seqs, slots), F32)
    for b in range(seqs):
        s = lax.dot_general(q, kb[b], (((1,), (1,)), ((), ())), preferred_element_type=F32)
        scores = jnp.where(row == b, s, scores)
    scores = scores * DH ** (-0.5) + bias[0]
    take, rest = log_sigmoids(scores)
    rest = jnp.where(visible, rest, 0.0)
    hi = rest.astype(BF16)
    left = rest - hi.astype(F32)
    lo = left.astype(BF16)
    last = (left - lo.astype(F32)).astype(BF16)
    t = tri[...]
    between = (
        jnp.dot(hi, t, preferred_element_type=F32)
        + jnp.dot(lo, t, preferred_element_type=F32)
        + jnp.dot(last, t, preferred_element_type=F32)
    )
    stick = jnp.where(visible, jnp.exp(take + between), 0.0)
    att = jnp.zeros((seqs, DH), F32)
    for b in range(seqs):
        only = jnp.where(row == b, stick, 0.0).astype(BF16)
        att = att + jnp.dot(only, vb[b], preferred_element_type=F32)
    att = att.astype(BF16)
    proj = jnp.dot(att, ow[...], preferred_element_type=F32)
    for k in range(kt):
        asend[k] = proj[:, k * 128 : (k + 1) * 128].astype(BF16)
    put_tp(3, lambda f: asend.at[f // 2], arecv)
    arecv[me_t] = asend[my_k]

    arrived(2, kvrecv, ep_n - 1)
    fresh = jnp.sum(kvrecv[:, 0].astype(F32), axis=0).astype(BF16).astype(F32)
    ms = jnp.mean(fresh * fresh, axis=-1, keepdims=True)
    keys_out[...] = (fresh * lax.rsqrt(ms + EPS)).astype(BF16)
    values_out[...] = jnp.sum(kvrecv[:, 1].astype(F32), axis=0).astype(BF16)

    arrived(3, arecv, tp_n - 1)
    middle = (tiles[my_k] + jnp.sum(arecv[...].astype(F32), axis=0)).astype(BF16)
    mid[my_k] = middle
    middle = middle.astype(F32)
    slot_row = lax.broadcasted_iota(jnp.int32, (2 * ep_n, 128), 0)
    outbox = jnp.zeros((2 * ep_n, 128), F32)
    for i in range(2 * seqs):
        b = i // 2
        outbox = jnp.where(slot_row == places[i] * ep_n + ids[i], middle[b : b + 1, :], outbox)
    xo[...] = outbox
    for e in range(ep_n):
        obox[e, :, 0:128] = xo[e : e + 1, :]
        obox[e, :, 128:256] = xo[ep_n + e : ep_n + e + 1, :]
    put_ep(4, lambda f: obox.at[f], ibox)
    put_tiles(5, mid)
    ibox[me_e] = obox[me_e]

    for i in (9, 10, 11, 12, 13):
        copies[i].wait()
    arrived(5, mid, 2 * yn - 1)
    ss = jnp.zeros((seqs, 128), F32)
    for k in range(kt):
        m = mid[k].astype(F32)
        ss = ss + m * m
    scale = lax.rsqrt(jnp.sum(ss, axis=-1, keepdims=True) * (1.0 / width) + EPS)
    gate = jnp.zeros((seqs, 128), F32)
    for k in range(kt):
        at = slice(k * 128, (k + 1) * 128)
        n = (mid[k].astype(F32) * scale * mgain[:, at]).astype(BF16)
        nmix[:, at] = n
        gate = gate + n.astype(F32) * bg[:, at]
    switch = jax.nn.sigmoid(jnp.sum(gate, axis=-1, keepdims=True))
    n = nmix[...]
    g = jnp.dot(n, sg[...], preferred_element_type=F32)
    u = jnp.dot(n, su[...], preferred_element_type=F32)
    hidden = (g * jax.nn.sigmoid(g) * u).astype(BF16)
    sout = jnp.dot(hidden, sd[...], preferred_element_type=F32)
    for k in range(kt):
        ssend[k] = sout[:, k * 128 : (k + 1) * 128].astype(BF16)
    put_tp(6, lambda f: ssend.at[f // 2], srecv)
    srecv[me_t] = ssend[my_k]

    for i in (14, 15, 16):
        copies[i].wait()
    arrived(4, ibox, ep_n - 1)
    for e in range(ep_n):
        xt[e : e + 1, :] = ibox[e, :, 0:128]
        xt[ep_n + e : ep_n + e + 1, :] = ibox[e, :, 128:256]
    xg[my_k] = xt[...].astype(BF16)
    put_tiles(7, xg)
    arrived(7, xg, 2 * yn - 1)
    ss = jnp.zeros((2 * ep_n, 128), F32)
    for k in range(kt):
        m = xg[k].astype(F32)
        ss = ss + m * m
    scale = lax.rsqrt(jnp.sum(ss, axis=-1, keepdims=True) * (1.0 / width) + EPS)
    for k in range(kt):
        at = slice(k * 128, (k + 1) * 128)
        xn[:, at] = (xg[k].astype(F32) * scale * mgain[:, at]).astype(BF16)
    x = xn[...]
    g = jnp.dot(x, eg[...], preferred_element_type=F32)
    u = jnp.dot(x, eu[...], preferred_element_type=F32)
    hidden = (g * jax.nn.sigmoid(g) * u).astype(BF16)
    lane = lax.broadcasted_iota(jnp.int32, (ep_n, 128), 1)
    for k in range(kt):
        at = slice(k * 128, (k + 1) * 128)
        out = jnp.dot(hidden, ed[:, at], preferred_element_type=F32)
        first, second = out[:ep_n], out[ep_n:]
        esend[2 * k] = jnp.where(lane < 64, first, pltpu.roll(second, 64, 1)).astype(BF16)
        esend[2 * k + 1] = jnp.where(lane < 64, pltpu.roll(first, 64, 1), second).astype(BF16)
    put_tp(8, lambda f: esend.at[f], erecv)
    erecv[me_t] = esend[me_t]
    arrived(6, srecv, tp_n - 1)
    base = middle + switch * jnp.sum(srecv[...].astype(F32), axis=0)
    base = jnp.where(side == 1, pltpu.roll(base, 64, 1), base)
    arrived(8, erecv, tp_n - 1)
    total = erecv[0].astype(F32)
    for j in range(1, tp_n):
        total = total + erecv[j].astype(F32)
    for e in range(ep_n):
        rsend[e] = total[e : e + 1, :]
    put_ep(9, lambda f: rsend.at[f], rrecv)
    rrecv[me_e] = rsend[me_e]
    arrived(9, rrecv, ep_n - 1)
    row = lax.broadcasted_iota(jnp.int32, (seqs, 128), 0)
    routed = jnp.zeros((seqs, 128), F32)
    for b in range(seqs):
        line = jnp.zeros((1, 128), F32)
        for k in range(2):
            got = rrecv[ids[2 * b + k]]
            got = jnp.where(places[2 * b + k] == 1, pltpu.roll(got, 64, 1), got)
            line = line + rweights[b, k] * got
        routed = jnp.where(row == b, line, routed)
    mixed_out[...] = (base + routed)[:, :64].astype(BF16)

    sent(0, nrecv, ep_n - 1)
    sent(1, qrecv, ep_n - 1)
    sent(2, kvrecv, ep_n - 1)
    sent(3, arecv, tp_n - 1)
    sent(4, ibox, ep_n - 1)
    sent(5, mid, 2 * yn - 1)
    sent(6, srecv, tp_n - 1)
    sent(7, xg, 2 * yn - 1)
    sent(8, erecv, tp_n - 1)
    sent(9, rrecv, ep_n - 1)


def body(
    ep_n,
    tp_n,
    tokens,
    attn_gain,
    query_weight,
    key_weight,
    value_weight,
    query_gain,
    stick_bias,
    key_cache,
    value_cache,
    lengths,
    out_weight,
    mix_gain,
    route_ids,
    route_weights,
    expert_gate,
    expert_up,
    expert_down,
    side_gate,
    side_up,
    side_down,
    branch_gate,
):
    seqs, width = tokens.shape
    slots = key_cache.shape[2]
    kt = width // 128
    any_ = pl.BlockSpec(memory_space=pl.ANY)
    smem = pl.BlockSpec(memory_space=pltpu.SMEM)
    vmem = pl.BlockSpec(memory_space=pltpu.VMEM)
    specs = [any_] * 21
    for i in (6, 9, 12, 13):
        specs[i] = smem
    V = pltpu.VMEM
    scratch = [
        V((seqs, width), BF16),
        V((1, width), F32),
        V((1, width), F32),
        V((1, DH), F32),
        V((1, width), F32),
        V((2 * query_weight.shape[0], 3 * DH), BF16),
        V((seqs, slots, DH), BF16),
        V((seqs, slots, DH), BF16),
        V(out_weight.shape, BF16),
        V(expert_gate.shape[1:], BF16),
        V(expert_up.shape[1:], BF16),
        V(expert_down.shape[1:], BF16),
        V(side_gate.shape, BF16),
        V(side_up.shape, BF16),
        V(side_down.shape, BF16),
        V((slots, slots), BF16),
        V((kt, seqs, 128), F32),
        V((kt, seqs, 128), BF16),
        V((ep_n, seqs, 128), BF16),
        V((ep_n, seqs, 128), BF16),
        V((ep_n, seqs, 128), BF16),
        V((ep_n, 2, seqs, 128), BF16),
        V((ep_n, 2, seqs, 128), BF16),
        V((kt, seqs, 128), BF16),
        V((tp_n, seqs, 128), BF16),
        V((kt, seqs, 128), BF16),
        V((seqs, width), BF16),
        V((2 * ep_n, 128), F32),
        V((ep_n, 1, 256), F32),
        V((ep_n, 1, 256), F32),
        V((2 * ep_n, 128), F32),
        V((kt, 2 * ep_n, 128), BF16),
        V((2 * ep_n, width), BF16),
        V((kt, seqs, 128), BF16),
        V((tp_n, seqs, 128), BF16),
        V((tp_n, ep_n, 128), BF16),
        V((tp_n, ep_n, 128), BF16),
        V((ep_n, 1, 128), F32),
        V((ep_n, 1, 128), F32),
        pltpu.SemaphoreType.DMA((17,)),
        pltpu.SemaphoreType.DMA((10,)),
        pltpu.SemaphoreType.DMA((10,)),
    ]
    return pl.pallas_call(
        functools.partial(kernel, ep_n, tp_n),
        out_shape=(
            jax.ShapeDtypeStruct((seqs, width // tp_n), BF16),
            jax.ShapeDtypeStruct((seqs, DH), BF16),
            jax.ShapeDtypeStruct((seqs, DH), BF16),
        ),
        in_specs=specs,
        out_specs=(vmem, vmem, vmem),
        scratch_shapes=scratch,
        compiler_params=pltpu.CompilerParams(
            collective_id=0, has_side_effects=True, vmem_limit_bytes=60 * 1024 * 1024
        ),
        name="decode_layer",
    )(
        tokens,
        attn_gain.reshape(1, -1),
        query_weight,
        key_weight,
        value_weight,
        query_gain.reshape(1, -1),
        stick_bias,
        key_cache,
        value_cache,
        lengths,
        out_weight,
        mix_gain.reshape(1, -1),
        route_ids,
        route_weights,
        expert_gate,
        expert_up,
        expert_down,
        side_gate,
        side_up,
        side_down,
        branch_gate.reshape(1, -1),
    )


def solution(mesh):
    in_specs = (
        P("ep", None),
        P(),
        P("ep", "tp"),
        P("ep", "tp"),
        P("ep", "tp"),
        P(),
        P("tp"),
        P("ep", "tp", None, None),
        P("ep", "tp", None, None),
        P("ep"),
        P("tp", None),
        P(),
        P("ep", None),
        P("ep", None),
        P("ep", None, "tp"),
        P("ep", None, "tp"),
        P("ep", "tp", None),
        P(None, "tp"),
        P(None, "tp"),
        P("tp", None),
        P(),
    )
    out_specs = (P("ep", "tp"), P("ep", "tp"), P("ep", "tp"))
    step = functools.partial(body, mesh.shape["ep"], mesh.shape["tp"])
    return jax.shard_map(step, mesh=mesh, in_specs=in_specs, out_specs=out_specs, check_vma=False)
```

time: 188 us -> 93 us (0.49)
  waiting for transfers between devices: 99.9 us -> 0 us
  Pallas kernels: 0 us -> 81.7 us
  starting transfers between devices: 33.6 us -> 0 us
  blocking collectives: 32.3 us -> 0 us
  other arithmetic: 9.51 us -> 0 us
  matrix products: 4.27 us -> 0 us
  local copies, waits for them, and re-layouts: 6.44 us -> 9.7 us
    all_to_all x5 -> x0, waiting for transfers between devices: 99.9 us -> none  [the longest x1 27.2 us: sum_at_owner(): lax.all_to_all(parts, axis, split_axis=0, concat_axis=0, tiled=True)]
    pallas_call x0 -> x1, Pallas kernels: none -> 81.7 us  [body(): pl.pallas_call(functools.partial(kernel, ep_n, tp_n), out_shape=(jax.Shap...]
    all_to_all x5 -> x0, starting transfers between devices: 33.6 us -> none  [the longest x1 9.8 us: copy_for_each(): return lax.all_to_all(copies, axis, split_axis=0, concat_axis=0, tiled=True)]
    all_to_all x1 -> x0, blocking collectives: 32.3 us -> none  [body(): lax.all_to_all(normed, 'ep', split_axis=1, concat_axis=0, tiled=True)]
    unnamed x36 -> x25, local copies, waits for them, and re-layouts: 0.45 us -> 9.7 us
    another operation x3 -> x0, other arithmetic: 5.03 us -> none
    dot_general x10 -> x0, matrix products: 4.27 us -> none  [the longest x1 1.68 us: body(): jnp.dot(picked, stacked, preferred_element_type=jnp.float32)]
    convert_element_type x5 -> x0, other arithmetic: 2.32 us -> none  [the longest x1 0.84 us: body(): normed = rms_scale(stream, attn_gain).astype(jnp.bfloat16)]
  transfers between devices with their start and end apart: 5 -> 0, of which waited for: 5 -> 0; matrix products, arithmetic and copies ran while one was open for 1% -> 0% of each run, Pallas kernels for 0% -> 0%
where the time goes in v1:
time: 93 us; the launch traced here: 92.7 us
  Pallas kernels  81.7 us (88%)
  local copies, waits for them, and re-layouts  9.7 us (10%)
  between operations  1.31 us (1%)
    pallas_call x1, Pallas kernels, body(): pl.pallas_call(functools.partial(kernel, ep_n, tp_n), out_shape=(jax.Shap...  81.7 us
    unnamed x25, local copies, waits for them, and re-layouts  9.7 us

profile of v1, /device:TPU:1, one launch (start us, length us, event | category | flops | bytes accessed | tf_op | source)
XLA Modules:
  0.0 92.7 jit_solution(16428601657377109780)
XLA Ops:
  1.3 0.0 copy-start.6
  1.3 0.7 copy-done.6
  2.0 0.0 copy-start.7
  2.0 0.7 copy.24.rids
  2.6 0.0 copy-done.7
  2.6 0.7 copy.25.rweights
  3.3 0.0 copy-start
  3.3 2.0 %copy.26.egate = bf16[1,2048,80]{2,1,0:T(8,128)(2,1)} copy(bf16[1,2048,80]{1,2,0:T(8,128)(2,1)} %param.35) | data formatting | bytes 655360 | tf_op args[14]
  5.3 0.0 copy-done
  5.3 0.0 copy-start.1
  5.3 1.0 %copy.27.eup = bf16[1,2048,80]{2,1,0:T(8,128)(2,1)} copy(bf16[1,2048,80]{1,2,0:T(8,128)(2,1)S(1)} %copy-done) | data formatting | bytes 655360 | tf_op args[15]
  6.4 0.0 copy-done.1
  6.4 0.0 copy-start.2
  6.4 1.0 %copy.28.sgate = bf16[2048,32]{1,0:T(8,128)(2,1)} copy(bf16[2048,32]{0,1:T(8,128)(2,1)S(1)} %copy-done.1) | data formatting | bytes 262144 | tf_op args[17]
  7.4 0.0 copy-done.2
  7.4 1.0 %copy.29.sup = bf16[2048,32]{1,0:T(8,128)(2,1)} copy(bf16[2048,32]{0,1:T(8,128)(2,1)S(1)} %copy-done.2) | data formatting | bytes 262144 | tf_op args[18]
  8.4 81.7 %decode_layer.1 = (bf16[8,64]{1,0:T(8,128)(2,1)}, bf16[8,128]{1,0:T(8,128)(2,1)}, bf16[8,128]{1,0:T(8,128)(2,1)}) custom-call(bf16[8,2048]{1,0:T(8,128)(2,1)} %tokens.1, f32[1,2048]{1,0:T(1,128)} %bitcast.4, bf16[64,128]{1,0:T(8,128)(2,1)} %wq.1, bf16[64,128]{1,0:T(8,128)(2,1)} %wk.1, bf16[64,128]{1,0:T(8,128)(2,1)} %wv.1, f32[1,128]{1,0:T(1,128)} %bitcast.7, ...), custom_call_target="tpu_custom_call" | custom-call | tf_op jit(solution)/shard_map/decode_layer/pallas_call | solution.py:489
  90.1 0.0 copy-start.5
  90.1 0.7 copy-done.5
  90.7 0.0 copy-start.4
  90.7 0.6 copy.34
  91.3 0.1 copy-done.4
  91.4 0.0 copy-start.3
  91.4 0.6 copy.35
  92.0 0.1 copy-done.3
  92.1 0.6 copy.36
Async XLA Ops:
  1.3 0.7 copy-start.6
  2.0 0.7 copy-start.7
  3.3 2.0 %copy-start = (bf16[1,2048,80]{1,2,0:T(8,128)(2,1)S(1)}, bf16[1,2048,80]{1,2,0:T(8,128)(2,1)}, u32[]{:S(2)}) copy-start(bf16[1,2048,80]{1,2,0:T(8,128)(2,1)} %param.36) | copy-start | bytes 983044
  5.3 1.0 %copy-start.1 = (bf16[2048,32]{0,1:T(8,128)(2,1)S(1)}, bf16[2048,32]{0,1:T(8,128)(2,1)}, u32[]{:S(2)}) copy-start(bf16[2048,32]{0,1:T(8,128)(2,1)} %param.38) | copy-start | bytes 393220
  6.4 1.0 %copy-start.2 = (bf16[2048,32]{0,1:T(8,128)(2,1)S(1)}, bf16[2048,32]{0,1:T(8,128)(2,1)}, u32[]{:S(2)}) copy-start(bf16[2048,32]{0,1:T(8,128)(2,1)} %param.39) | copy-start | bytes 393220
  90.1 0.7 copy-start.5
  90.7 0.7 copy-start.4
  91.4 0.7 copy-start.3

commit v2 on v1

--- a/solution.py
+++ b/solution.py
@@ -17,7 +17,11 @@
 
 def far_first(i, n):
     half = (i + 1) // 2
-    return n // 2 + half * (2 * lax.rem(i + 1, 2) - 1)
+    return n // 2 - half * (2 * lax.rem(i + 1, 2) - 1)
+
+
+def dot_t(a, b):
+    return lax.dot_general(a, b, (((1,), (1,)), ((), ())), preferred_element_type=F32)
 
 
 def log_sigmoids(x):
@@ -37,11 +41,11 @@
     bias,
     kcache,
     vcache,
-    lengths,
+    lengths_in,
     oweight,
     mix_gain,
-    rids,
-    rweights,
+    rids_in,
+    rweights_in,
     egate,
     eup,
     edown,
@@ -71,8 +75,6 @@
     tiles,
     nsend,
     nrecv,
-    qsend,
-    qrecv,
     kvsend,
     kvrecv,
     asend,
@@ -91,9 +93,18 @@
     erecv,
     rsend,
     rrecv,
+    wall,
+    lengths,
+    rids,
+    rweights,
+    far,
+    parts,
+    back,
     ld,
     snd,
     rcv,
+    wsnd,
+    wrcv,
 ):
     me_e = lax.axis_index("ep")
     me_t = lax.axis_index("tp")
@@ -117,12 +128,23 @@
 
     barrier = pltpu.get_barrier_semaphore()
 
+    def along(k):
+        return lax.rem(me_e + 2 * k + ep_n, ep_n)
+
+    def tell(sem, dest):
+        pl.semaphore_signal(sem, inc=1, device_id=dest, device_id_type=MESH)
+
+    near = ep_n // 8
+    zs = ep_n // 2
+    my_z = me_e // 2
+    partner = {"ep": me_e + 1 - 2 * core}
+
     def greet_ep(i, c):
-        pl.semaphore_signal(barrier, inc=1, device_id={"ep": ep_peer(i)}, device_id_type=MESH)
+        tell(barrier, {"ep": ep_peer(i)})
         return c
 
     def greet_tp(i, c):
-        pl.semaphore_signal(barrier, inc=1, device_id={"tp": tp_peer(i)}, device_id_type=MESH)
+        tell(barrier, {"tp": tp_peer(i)})
         return c
 
     lax.fori_loop(0, ep_n - 1, greet_ep, 0)
@@ -133,9 +155,9 @@
     loads = [
         (tokens, tok),
         (attn_gain, again),
-        (wq, wpad.at[at_w, pl.ds(0, DH)]),
-        (wk, wpad.at[at_w, pl.ds(DH, DH)]),
-        (wv, wpad.at[at_w, pl.ds(2 * DH, DH)]),
+        (wq, wall.at[me_e]),
+        (wk, wpad.at[at_w, pl.ds(0, DH)]),
+        (wv, wpad.at[at_w, pl.ds(DH, DH)]),
         (qgain, qg),
         (kcache.at[:, 0], kb),
         (vcache.at[:, 0], vb),
@@ -148,25 +170,22 @@
         (egate.at[0], eg),
         (eup.at[0], eu),
         (edown.at[0], ed),
+        (lengths_in, lengths),
+        (rids_in, rids),
+        (rweights_in, rweights),
     ]
     copies = [pltpu.make_async_copy(a, b, ld.at[i]) for i, (a, b) in enumerate(loads)]
-    for c in copies:
-        c.start()
+    for i in (2, 0, 1):
+        copies[i].start()
+    for i, c in enumerate(copies):
+        if i > 2:
+            c.start()
 
     other = pl.ds(pl.multiple_of((1 - core) * rows_w, rows_w), rows_w)
-    wpad[other, :] = jnp.zeros((rows_w, 3 * DH), BF16)
+    wpad[other, :] = jnp.zeros((rows_w, 2 * DH), BF16)
     r_i = lax.broadcasted_iota(jnp.int32, (slots, slots), 0)
     c_i = lax.broadcasted_iota(jnp.int32, (slots, slots), 1)
     tri[...] = jnp.where(r_i > c_i, 1.0, 0.0).astype(BF16)
-
-    ids = [rids[b, k] for b in range(seqs) for k in range(2)]
-    places = []
-    for i in range(2 * seqs):
-        n = jnp.int32(0)
-        for j in range(i):
-            if j // 2 != i // 2:
-                n = n + jnp.where(ids[j] == ids[i], 1, 0)
-        places.append(n)
 
     copies[0].wait()
     copies[1].wait()
@@ -177,15 +196,48 @@
         tiles[k] = stream[:, k * 128 : (k + 1) * 128]
         nsend[k] = normed[:, k * 128 : (k + 1) * 128]
     nrecv[me_e] = nsend[me_e // 2]
-
+    copies[2].wait()
     pl.semaphore_wait(barrier, ep_n + tp_n - 2)
 
-    def put_ep(p, src_of, dst):
+    def put_block(dest, block, p, sem):
+        pltpu.make_async_remote_copy(
+            src_ref=wall.at[block],
+            dst_ref=wall.at[block],
+            send_sem=wsnd.at[p],
+            recv_sem=sem,
+            device_id=dest,
+            device_id_type=MESH,
+        ).start()
+
+    def chip_at(d):
+        return lax.rem(my_z + d + zs, zs)
+
+    def put_far(dest, d, slot):
+        pltpu.make_async_remote_copy(
+            src_ref=nsend.at[chip_at(d)],
+            dst_ref=far.at[slot],
+            send_sem=snd.at[1],
+            recv_sem=rcv.at[1],
+            device_id={"ep": dest},
+            device_id_type=MESH,
+        ).start()
+
+    for k in range(near, 0, -1):
+        put_block({"ep": along(-k)}, me_e, 0, wrcv.at[me_e])
+        put_block({"ep": along(k)}, me_e, 0, wrcv.at[me_e])
+        if k == near:
+            put_block(partner, me_e, 1, wrcv.at[ep_n])
+            for d in range(1, near + 1):
+                put_far(along(near), near + d, d - 1)
+            for d in range(1, near):
+                put_far(along(-near), -near - d, near + d - 1)
+
+    def put_ep(p, src_of, dst, first=0, end=ep_n - 1, place=lambda i: me_e, peer=ep_peer):
         def one(i, c):
-            f = ep_peer(i)
+            f = peer(i)
             pltpu.make_async_remote_copy(
                 src_ref=src_of(f),
-                dst_ref=dst.at[me_e],
+                dst_ref=dst.at[place(i)],
                 send_sem=snd.at[p],
                 recv_sem=rcv.at[p],
                 device_id={"ep": f},
@@ -193,7 +245,7 @@
             ).start()
             return c
 
-        lax.fori_loop(0, ep_n - 1, one, 0)
+        lax.fori_loop(first, end, one, 0)
 
     def put_tp(p, src_of, dst):
         def one(i, c):
@@ -235,22 +287,16 @@
         part = buf.at[pl.ds(0, n)]
         pltpu.make_async_copy(part, part, snd.at[p]).wait()
 
-    put_ep(0, lambda f: nsend.at[f // 2], nrecv)
-    for i in (2, 3, 4, 5):
+    for i in (17, 18, 19):
         copies[i].wait()
-    arrived(0, nrecv, ep_n - 1)
-    picked = nrecv[...].astype(F32).reshape(ep_n * seqs, 128).astype(BF16)
-    part = jnp.dot(picked, wpad[:, :DH], preferred_element_type=F32)
-    for f in range(ep_n):
-        qsend[f] = part[f * seqs : (f + 1) * seqs].astype(BF16)
-    put_ep(1, lambda f: qsend.at[f], qrecv)
-    qrecv[me_e] = qsend[me_e]
-    part = jnp.dot(picked, wpad[:, DH:], preferred_element_type=F32)
-    for f in range(ep_n):
-        kvsend[f, 0] = part[f * seqs : (f + 1) * seqs, :DH].astype(BF16)
-        kvsend[f, 1] = part[f * seqs : (f + 1) * seqs, DH:].astype(BF16)
-    put_ep(2, lambda f: kvsend.at[f], kvrecv)
-    kvrecv[me_e] = kvsend[me_e]
+    ids = [rids[k, b] for b in range(seqs) for k in range(2)]
+    places = []
+    for i in range(2 * seqs):
+        n = jnp.int32(0)
+        for j in range(i):
+            if j // 2 != i // 2:
+                n = n + jnp.where(ids[j] == ids[i], 1, 0)
+        places.append(n)
 
     row = lax.broadcasted_iota(jnp.int32, (seqs, slots), 0)
     pos = lax.broadcasted_iota(jnp.int32, (seqs, slots), 1)
@@ -258,16 +304,62 @@
     for b in range(seqs):
         lens = jnp.where(row == b, lengths[b], lens)
     visible = pos < lens
-    copies[6].wait()
-    copies[7].wait()
-    copies[8].wait()
-    arrived(1, qrecv, ep_n - 1)
-    q = jnp.sum(qrecv[...].astype(F32), axis=0).astype(BF16).astype(F32)
+    for i in (5, 6, 7, 8):
+        copies[i].wait()
+
+    def block_came(block):
+        pltpu.make_async_copy(wall.at[block], wall.at[block], wrcv.at[block]).wait()
+        put_block(partner, block, 1, wrcv.at[ep_n])
+
+    for k in range(1, near + 1):
+        block_came(along(-k))
+        block_came(along(k))
+    arrived(1, far, 2 * near - 1)
+    theirs = wall.at[pl.ds(0, 2 * near + 1)]
+    pltpu.make_async_copy(theirs, theirs, wrcv.at[ep_n]).wait()
+
+    def times_block(rows, d):
+        block = wall[pl.ds(2 * chip_at(d), 2)].reshape(128, DH)
+        return jnp.dot(rows, block, preferred_element_type=F32)
+
+    q = times_block(nsend[chip_at(0)], 0)
+    from_low = jnp.zeros((seqs, DH), F32)
+    from_high = jnp.zeros((seqs, DH), F32)
+    for d in range(1, near + 1):
+        both = jnp.concatenate([nsend[chip_at(d)], far[d - 1]], axis=0)
+        both = times_block(both, d)
+        q = q + both[:seqs]
+        from_low = from_low + both[seqs:]
+        if d < near:
+            both = jnp.concatenate([nsend[chip_at(-d)], far[near + d - 1]], axis=0)
+            both = times_block(both, -d)
+            q = q + both[:seqs]
+            from_high = from_high + both[seqs:]
+        else:
+            q = q + times_block(nsend[chip_at(-d)], -d)
+    parts[0] = from_low
+    parts[1] = from_high
+
+    def put_part(dest, slot):
+        pltpu.make_async_remote_copy(
+            src_ref=parts.at[slot],
+            dst_ref=back.at[slot],
+            send_sem=wsnd.at[2],
+            recv_sem=wrcv.at[ep_n + 1],
+            device_id={"ep": dest},
+            device_id_type=MESH,
+        ).start()
+
+    put_part(along(-near), 0)
+    put_part(along(near), 1)
+    pltpu.make_async_copy(back, back, wrcv.at[ep_n + 1]).wait()
+    q = q + back[0] + back[1]
+    q = q.astype(BF16).astype(F32)
     ms = jnp.mean(q * q, axis=-1, keepdims=True)
     q = (q * lax.rsqrt(ms + EPS) * qg[...]).astype(BF16)
     scores = jnp.zeros((seqs, slots), F32)
     for b in range(seqs):
-        s = lax.dot_general(q, kb[b], (((1,), (1,)), ((), ())), preferred_element_type=F32)
+        s = dot_t(q, kb[b])
         scores = jnp.where(row == b, s, scores)
     scores = scores * DH ** (-0.5) + bias[0]
     take, rest = log_sigmoids(scores)
@@ -294,11 +386,7 @@
     put_tp(3, lambda f: asend.at[f // 2], arecv)
     arecv[me_t] = asend[my_k]
 
-    arrived(2, kvrecv, ep_n - 1)
-    fresh = jnp.sum(kvrecv[:, 0].astype(F32), axis=0).astype(BF16).astype(F32)
-    ms = jnp.mean(fresh * fresh, axis=-1, keepdims=True)
-    keys_out[...] = (fresh * lax.rsqrt(ms + EPS)).astype(BF16)
-    values_out[...] = jnp.sum(kvrecv[:, 1].astype(F32), axis=0).astype(BF16)
+    put_ep(0, lambda f: nsend.at[f // 2], nrecv)
 
     arrived(3, arecv, tp_n - 1)
     middle = (tiles[my_k] + jnp.sum(arecv[...].astype(F32), axis=0)).astype(BF16)
@@ -313,9 +401,16 @@
     for e in range(ep_n):
         obox[e, :, 0:128] = xo[e : e + 1, :]
         obox[e, :, 128:256] = xo[ep_n + e : ep_n + e + 1, :]
-    put_ep(4, lambda f: obox.at[f], ibox)
+    half = ep_n // 2
+    quarter = ep_n // 4
+
+    def offset(i):
+        return lax.rem(ep_n + quarter - far_first(i, ep_n), ep_n)
+
+    put_ep(4, lambda f: obox.at[f], ibox, 0, half, offset)
+    put_ep(10, lambda f: obox.at[f], ibox, half, ep_n - 1, offset)
     put_tiles(5, mid)
-    ibox[me_e] = obox[me_e]
+    ibox[quarter] = obox[me_e]
 
     for i in (9, 10, 11, 12, 13):
         copies[i].wait()
@@ -333,8 +428,8 @@
         gate = gate + n.astype(F32) * bg[:, at]
     switch = jax.nn.sigmoid(jnp.sum(gate, axis=-1, keepdims=True))
     n = nmix[...]
-    g = jnp.dot(n, sg[...], preferred_element_type=F32)
-    u = jnp.dot(n, su[...], preferred_element_type=F32)
+    g = dot_t(n, sg[...])
+    u = dot_t(n, su[...])
     hidden = (g * jax.nn.sigmoid(g) * u).astype(BF16)
     sout = jnp.dot(hidden, sd[...], preferred_element_type=F32)
     for k in range(kt):
@@ -344,45 +439,85 @@
 
     for i in (14, 15, 16):
         copies[i].wait()
-    arrived(4, ibox, ep_n - 1)
-    for e in range(ep_n):
-        xt[e : e + 1, :] = ibox[e, :, 0:128]
-        xt[ep_n + e : ep_n + e + 1, :] = ibox[e, :, 128:256]
-    xg[my_k] = xt[...].astype(BF16)
-    put_tiles(7, xg)
-    arrived(7, xg, 2 * yn - 1)
-    ss = jnp.zeros((2 * ep_n, 128), F32)
-    for k in range(kt):
-        m = xg[k].astype(F32)
-        ss = ss + m * m
-    scale = lax.rsqrt(jnp.sum(ss, axis=-1, keepdims=True) * (1.0 / width) + EPS)
-    for k in range(kt):
-        at = slice(k * 128, (k + 1) * 128)
-        xn[:, at] = (xg[k].astype(F32) * scale * mgain[:, at]).astype(BF16)
-    x = xn[...]
-    g = jnp.dot(x, eg[...], preferred_element_type=F32)
-    u = jnp.dot(x, eu[...], preferred_element_type=F32)
-    hidden = (g * jax.nn.sigmoid(g) * u).astype(BF16)
-    lane = lax.broadcasted_iota(jnp.int32, (ep_n, 128), 1)
-    for k in range(kt):
-        at = slice(k * 128, (k + 1) * 128)
-        out = jnp.dot(hidden, ed[:, at], preferred_element_type=F32)
-        first, second = out[:ep_n], out[ep_n:]
-        esend[2 * k] = jnp.where(lane < 64, first, pltpu.roll(second, 64, 1)).astype(BF16)
-        esend[2 * k + 1] = jnp.where(lane < 64, pltpu.roll(first, 64, 1), second).astype(BF16)
-    put_tp(8, lambda f: esend.at[f], erecv)
-    erecv[me_t] = esend[me_t]
+    def pass_on(g, p):
+        for r in range(half):
+            xt[r : r + 1, :] = ibox[g * half + r, :, 0:128]
+            xt[half + r : half + r + 1, :] = ibox[g * half + r, :, 128:256]
+        xg[g, my_k] = xt[...].astype(BF16)
+        put_tiles(p, xg.at[g])
+
+    arrived(10, ibox, half - 1)
+    pass_on(0, 7)
+    arrived(4, ibox, half)
+    pass_on(1, 11)
+
+    copies[3].wait()
+    copies[4].wait()
+    arrived(0, nrecv, ep_n - 1)
+    picked = nrecv[...].astype(F32).reshape(ep_n * seqs, 128).astype(BF16)
+    part = jnp.dot(picked, wpad[...], preferred_element_type=F32)
+    for f in range(ep_n):
+        kvsend[f, 0] = part[f * seqs : (f + 1) * seqs, :DH].astype(BF16)
+        kvsend[f, 1] = part[f * seqs : (f + 1) * seqs, DH:].astype(BF16)
+    put_ep(2, lambda f: kvsend.at[f], kvrecv)
+    kvrecv[me_e] = kvsend[me_e]
+
+    lane = lax.broadcasted_iota(jnp.int32, (half, 128), 1)
+
+    def expert(g, p, q):
+        arrived(p, xg.at[g], 2 * yn - 1)
+        ss = jnp.zeros((ep_n, 128), F32)
+        for k in range(kt):
+            m = xg[g, k].astype(F32)
+            ss = ss + m * m
+        scale = lax.rsqrt(jnp.sum(ss, axis=-1, keepdims=True) * (1.0 / width) + EPS)
+        for k in range(kt):
+            at = slice(k * 128, (k + 1) * 128)
+            xn[:, at] = (xg[g, k].astype(F32) * scale * mgain[:, at]).astype(BF16)
+        x = xn[...]
+        a = dot_t(x, eg[...])
+        u = dot_t(x, eu[...])
+        hidden = (a * jax.nn.sigmoid(a) * u).astype(BF16)
+        for k in range(kt):
+            at = slice(k * 128, (k + 1) * 128)
+            out = jnp.dot(hidden, ed[:, at], preferred_element_type=F32)
+            top, low = out[:half], out[half:]
+            esend[g, 2 * k] = jnp.where(lane < 64, top, pltpu.roll(low, 64, 1)).astype(BF16)
+            esend[g, 2 * k + 1] = jnp.where(lane < 64, pltpu.roll(top, 64, 1), low).astype(BF16)
+        put_tp(q, lambda f: esend.at[g, f], erecv.at[g])
+        erecv[g, me_t] = esend[g, me_t]
+
+    expert(0, 7, 8)
+    expert(1, 11, 12)
+    arrived(2, kvrecv, ep_n - 1)
+    fresh = jnp.sum(kvrecv[:, 0].astype(F32), axis=0).astype(BF16).astype(F32)
+    ms = jnp.mean(fresh * fresh, axis=-1, keepdims=True)
+    keys_out[...] = (fresh * lax.rsqrt(ms + EPS)).astype(BF16)
+    values_out[...] = jnp.sum(kvrecv[:, 1].astype(F32), axis=0).astype(BF16)
+
     arrived(6, srecv, tp_n - 1)
     base = middle + switch * jnp.sum(srecv[...].astype(F32), axis=0)
     base = jnp.where(side == 1, pltpu.roll(base, 64, 1), base)
-    arrived(8, erecv, tp_n - 1)
-    total = erecv[0].astype(F32)
-    for j in range(1, tp_n):
-        total = total + erecv[j].astype(F32)
-    for e in range(ep_n):
-        rsend[e] = total[e : e + 1, :]
-    put_ep(9, lambda f: rsend.at[f], rrecv)
-    rrecv[me_e] = rsend[me_e]
+
+    def give_back(g, p, first, end):
+        arrived(p, erecv.at[g], tp_n - 1)
+        total = erecv[g, 0].astype(F32)
+        for j in range(1, tp_n):
+            total = total + erecv[g, j].astype(F32)
+        for r in range(half):
+            rsend[g * half + r] = total[r : r + 1, :]
+
+        def back_offset(f):
+            return lax.rem(f - me_e + quarter + ep_n, ep_n)
+
+        def source(i):
+            return lax.rem(me_e + ep_n - far_first(i, ep_n), ep_n)
+
+        put_ep(9, lambda f: rsend.at[back_offset(f)], rrecv, first, end, peer=source)
+
+    give_back(0, 8, half, ep_n - 1)
+    give_back(1, 12, 0, half)
+    rrecv[me_e] = rsend[quarter]
     arrived(9, rrecv, ep_n - 1)
     row = lax.broadcasted_iota(jnp.int32, (seqs, 128), 0)
     routed = jnp.zeros((seqs, 128), F32)
@@ -391,20 +526,37 @@
         for k in range(2):
             got = rrecv[ids[2 * b + k]]
             got = jnp.where(places[2 * b + k] == 1, pltpu.roll(got, 64, 1), got)
-            line = line + rweights[b, k] * got
+            line = line + rweights[k, b] * got
         routed = jnp.where(row == b, line, routed)
     mixed_out[...] = (base + routed)[:, :64].astype(BF16)
 
     sent(0, nrecv, ep_n - 1)
-    sent(1, qrecv, ep_n - 1)
+    sent(1, far, 2 * near - 1)
+    others = wall.at[pl.ds(0, 2 * near)]
+    pltpu.make_async_copy(others, others, wsnd.at[0]).wait()
+    pltpu.make_async_copy(theirs, theirs, wsnd.at[1]).wait()
+    pltpu.make_async_copy(back, back, wsnd.at[2]).wait()
     sent(2, kvrecv, ep_n - 1)
     sent(3, arecv, tp_n - 1)
-    sent(4, ibox, ep_n - 1)
+    sent(4, ibox, half)
+    sent(10, ibox, half - 1)
     sent(5, mid, 2 * yn - 1)
     sent(6, srecv, tp_n - 1)
-    sent(7, xg, 2 * yn - 1)
-    sent(8, erecv, tp_n - 1)
+    for g in range(2):
+        sent((7, 11)[g], xg.at[g], 2 * yn - 1)
+        sent((8, 12)[g], erecv.at[g], tp_n - 1)
     sent(9, rrecv, ep_n - 1)
+
+
+def hand_over(a, b, c, x, y, z, sem):
+    copies = [
+        pltpu.make_async_copy(src, dst, sem.at[i])
+        for i, (src, dst) in enumerate(((a, x), (b, y), (c, z)))
+    ]
+    for one in copies:
+        one.start()
+    for one in copies:
+        one.wait()
 
 
 def body(
@@ -436,11 +588,9 @@
     slots = key_cache.shape[2]
     kt = width // 128
     any_ = pl.BlockSpec(memory_space=pl.ANY)
-    smem = pl.BlockSpec(memory_space=pltpu.SMEM)
     vmem = pl.BlockSpec(memory_space=pltpu.VMEM)
     specs = [any_] * 21
-    for i in (6, 9, 12, 13):
-        specs[i] = smem
+    specs[6] = pl.BlockSpec(memory_space=pltpu.SMEM)
     V = pltpu.VMEM
     scratch = [
         V((seqs, width), BF16),
@@ -448,21 +598,19 @@
         V((1, width), F32),
         V((1, DH), F32),
         V((1, width), F32),
-        V((2 * query_weight.shape[0], 3 * DH), BF16),
+        V((2 * query_weight.shape[0], 2 * DH), BF16),
         V((seqs, slots, DH), BF16),
         V((seqs, slots, DH), BF16),
         V(out_weight.shape, BF16),
-        V(expert_gate.shape[1:], BF16),
-        V(expert_up.shape[1:], BF16),
+        V(expert_gate.shape[:0:-1], BF16),
+        V(expert_up.shape[:0:-1], BF16),
         V(expert_down.shape[1:], BF16),
-        V(side_gate.shape, BF16),
-        V(side_up.shape, BF16),
+        V(side_gate.shape[::-1], BF16),
+        V(side_up.shape[::-1], BF16),
         V(side_down.shape, BF16),
         V((slots, slots), BF16),
         V((kt, seqs, 128), F32),
         V((kt, seqs, 128), BF16),
-        V((ep_n, seqs, 128), BF16),
-        V((ep_n, seqs, 128), BF16),
         V((ep_n, seqs, 128), BF16),
         V((ep_n, 2, seqs, 128), BF16),
         V((ep_n, 2, seqs, 128), BF16),
@@ -473,26 +621,32 @@
         V((2 * ep_n, 128), F32),
         V((ep_n, 1, 256), F32),
         V((ep_n, 1, 256), F32),
-        V((2 * ep_n, 128), F32),
-        V((kt, 2 * ep_n, 128), BF16),
-        V((2 * ep_n, width), BF16),
+        V((ep_n, 128), F32),
+        V((2, kt, ep_n, 128), BF16),
+        V((ep_n, width), BF16),
         V((kt, seqs, 128), BF16),
         V((tp_n, seqs, 128), BF16),
-        V((tp_n, ep_n, 128), BF16),
-        V((tp_n, ep_n, 128), BF16),
+        V((2, tp_n, ep_n // 2, 128), BF16),
+        V((2, tp_n, ep_n // 2, 128), BF16),
         V((ep_n, 1, 128), F32),
         V((ep_n, 1, 128), F32),
-        pltpu.SemaphoreType.DMA((17,)),
-        pltpu.SemaphoreType.DMA((10,)),
-        pltpu.SemaphoreType.DMA((10,)),
+        V((ep_n, *query_weight.shape), BF16),
+        pltpu.SMEM((seqs,), jnp.int32),
+        pltpu.SMEM((2, seqs), jnp.int32),
+        pltpu.SMEM((2, seqs), F32),
+        V((ep_n // 4 - 1, seqs, 128), BF16),
+        V((2, seqs, DH), F32),
+        V((2, seqs, DH), F32),
+        pltpu.SemaphoreType.DMA((20,)),
+        pltpu.SemaphoreType.DMA((13,)),
+        pltpu.SemaphoreType.DMA((13,)),
+        pltpu.SemaphoreType.DMA((3,)),
+        pltpu.SemaphoreType.DMA((ep_n + 2,)),
     ]
-    return pl.pallas_call(
+    shapes = ((seqs, width // tp_n), (seqs, DH), (seqs, DH))
+    results = pl.pallas_call(
         functools.partial(kernel, ep_n, tp_n),
-        out_shape=(
-            jax.ShapeDtypeStruct((seqs, width // tp_n), BF16),
-            jax.ShapeDtypeStruct((seqs, DH), BF16),
-            jax.ShapeDtypeStruct((seqs, DH), BF16),
-        ),
+        out_shape=tuple(V(s, BF16) for s in shapes),
         in_specs=specs,
         out_specs=(vmem, vmem, vmem),
         scratch_shapes=scratch,
@@ -513,16 +667,24 @@
         lengths,
         out_weight,
         mix_gain.reshape(1, -1),
-        route_ids,
-        route_weights,
-        expert_gate,
-        expert_up,
+        route_ids.T,
+        route_weights.T,
+        jnp.swapaxes(expert_gate, 1, 2),
+        jnp.swapaxes(expert_up, 1, 2),
         expert_down,
-        side_gate,
-        side_up,
+        side_gate.T,
+        side_up.T,
         side_down,
         branch_gate.reshape(1, -1),
     )
+    return pl.pallas_call(
+        hand_over,
+        out_shape=tuple(jax.ShapeDtypeStruct(s, BF16) for s in shapes),
+        in_specs=[vmem] * 3,
+        out_specs=[any_] * 3,
+        scratch_shapes=[pltpu.SemaphoreType.DMA((3,))],
+        name="hand_over",
+    )(*[pltpu.with_memory_space_constraint(r, pltpu.VMEM) for r in results])
 
 
 def solution(mesh):

time: 93 us -> 77.1 us (0.83)
  local copies, waits for them, and re-layouts: 9.7 us -> 0 us
  Pallas kernels: 81.7 us -> 75.7 us
    unnamed x25 -> x0, local copies, waits for them, and re-layouts: 9.7 us -> none
    pallas_call x1 -> x2, Pallas kernels: 81.7 us -> 75.7 us  [the longest x1 75.1 us: body(): pl.pallas_call(functools.partial(kernel, ep_n, tp_n), out_shape=tuple((V(...]
where the time goes in v2:
time: 77.1 us; the launch traced here: 77 us
  Pallas kernels  75.7 us (98%)
  between operations  1.29 us (2%)
    pallas_call x1, Pallas kernels, body(): pl.pallas_call(functools.partial(kernel, ep_n, tp_n), out_shape=tuple((V(...  75.1 us

profile of v2, /device:TPU:1, one launch (start us, length us, event | category | flops | bytes accessed | tf_op | source)
XLA Modules:
  0.0 77.0 jit_solution(8850829798859195615)
XLA Ops:
  1.3 75.1 %decode_layer.1 = (bf16[8,64]{1,0:T(8,128)(2,1)S(1)}, bf16[8,128]{1,0:T(8,128)(2,1)S(1)}, bf16[8,128]{1,0:T(8,128)(2,1)S(1)}) custom-call(bf16[8,2048]{1,0:T(8,128)(2,1)} %tokens.1, f32[1,2048]{1,0:T(1,128)} %bitcast.14, bf16[64,128]{1,0:T(8,128)(2,1)} %wq.1, bf16[64,128]{1,0:T(8,128)(2,1)} %wk.1, bf16[64,128]{1,0:T(8,128)(2,1)} %wv.1, f32[1,128]{1,0:T(1,128)} %bitcast.19, ...), custom_call_target="tpu_custom_call" | custom-call | tf_op jit(solution)/shard_map/decode_layer/pallas_call | solution.py:647
  76.4 0.6 hand_over.1

commit v3 on v2

--- a/solution.py
+++ b/solution.py
@@ -100,6 +100,10 @@
     far,
     parts,
     back,
+    from_down,
+    from_up,
+    column_left,
+    column_right,
     ld,
     snd,
     rcv,
@@ -139,16 +143,15 @@
     my_z = me_e // 2
     partner = {"ep": me_e + 1 - 2 * core}
 
-    def greet_ep(i, c):
-        tell(barrier, {"ep": ep_peer(i)})
-        return c
-
-    def greet_tp(i, c):
-        tell(barrier, {"tp": tp_peer(i)})
-        return c
-
-    lax.fori_loop(0, ep_n - 1, greet_ep, 0)
-    lax.fori_loop(0, tp_n - 1, greet_tp, 0)
+    y_down = {"tp": lax.rem(my_y + yn - 1, yn) * XN + my_x}
+    y_up = {"tp": lax.rem(my_y + 1, yn) * XN + my_x}
+    x_left = {"tp": my_y * XN + lax.rem(my_x + XN - 1, XN)}
+    x_right = {"tp": my_y * XN + lax.rem(my_x + 1, XN)}
+    greeted = [partner, y_down, y_up, x_left, x_right]
+    for k in range(near, 0, -1):
+        greeted += [{"ep": along(-k)}, {"ep": along(k)}]
+    for dest in greeted:
+        tell(barrier, dest)
 
     rows_w = wq.shape[0]
     at_w = pl.ds(pl.multiple_of(core * rows_w, rows_w), rows_w)
@@ -197,7 +200,7 @@
         nsend[k] = normed[:, k * 128 : (k + 1) * 128]
     nrecv[me_e] = nsend[me_e // 2]
     copies[2].wait()
-    pl.semaphore_wait(barrier, ep_n + tp_n - 2)
+    pl.semaphore_wait(barrier, len(greeted))
 
     def put_block(dest, block, p, sem):
         pltpu.make_async_remote_copy(
@@ -231,6 +234,22 @@
                 put_far(along(near), near + d, d - 1)
             for d in range(1, near):
                 put_far(along(-near), -near - d, near + d - 1)
+
+    tell(from_down.at[2], y_up)
+    tell(from_up.at[2], y_down)
+    for k in range(2, yn // 2 + 1):
+        pl.semaphore_wait(from_down.at[k], 1)
+        if k < yn // 2:
+            tell(from_down.at[k + 1], y_up)
+            pl.semaphore_wait(from_up.at[k], 1)
+            if k < yn // 2 - 1:
+                tell(from_up.at[k + 1], y_down)
+    tell(column_left.at[0], x_right)
+    tell(column_right.at[0], x_left)
+    pl.semaphore_wait(column_left.at[0], 1)
+    tell(column_left.at[1], x_right)
+    pl.semaphore_wait(column_right.at[0], 1)
+    pl.semaphore_wait(column_left.at[1], 1)
 
     def put_ep(p, src_of, dst, first=0, end=ep_n - 1, place=lambda i: me_e, peer=ep_peer):
         def one(i, c):
@@ -368,12 +387,9 @@
     left = rest - hi.astype(F32)
     lo = left.astype(BF16)
     last = (left - lo.astype(F32)).astype(BF16)
-    t = tri[...]
-    between = (
-        jnp.dot(hi, t, preferred_element_type=F32)
-        + jnp.dot(lo, t, preferred_element_type=F32)
-        + jnp.dot(last, t, preferred_element_type=F32)
-    )
+    pieces = jnp.concatenate([hi.astype(F32), lo.astype(F32), last.astype(F32)], axis=0)
+    sums = jnp.dot(pieces.astype(BF16), tri[...], preferred_element_type=F32)
+    between = sums[:seqs] + sums[seqs : 2 * seqs] + sums[2 * seqs :]
     stick = jnp.where(visible, jnp.exp(take + between), 0.0)
     att = jnp.zeros((seqs, DH), F32)
     for b in range(seqs):
@@ -411,6 +427,27 @@
     put_ep(10, lambda f: obox.at[f], ibox, half, ep_n - 1, offset)
     put_tiles(5, mid)
     ibox[quarter] = obox[me_e]
+
+    copies[3].wait()
+    copies[4].wait()
+    arrived(0, nrecv, ep_n - 1)
+    picked = nrecv[...].astype(F32).reshape(ep_n * seqs, 128).astype(BF16)
+    part = jnp.dot(picked, wpad[...], preferred_element_type=F32)
+    for f in range(ep_n):
+        kvsend[f, 0] = part[f * seqs : (f + 1) * seqs, :DH].astype(BF16)
+        kvsend[f, 1] = part[f * seqs : (f + 1) * seqs, DH:].astype(BF16)
+
+    def pass_on(g, p):
+        for r in range(half):
+            xt[r : r + 1, :] = ibox[g * half + r, :, 0:128]
+            xt[half + r : half + r + 1, :] = ibox[g * half + r, :, 128:256]
+        xg[g, my_k] = xt[...].astype(BF16)
+        put_tiles(p, xg.at[g])
+
+    arrived(10, ibox, half - 1)
+    pass_on(0, 7)
+    arrived(4, ibox, half)
+    pass_on(1, 11)
 
     for i in (9, 10, 11, 12, 13):
         copies[i].wait()
@@ -436,32 +473,11 @@
         ssend[k] = sout[:, k * 128 : (k + 1) * 128].astype(BF16)
     put_tp(6, lambda f: ssend.at[f // 2], srecv)
     srecv[me_t] = ssend[my_k]
+    put_ep(2, lambda f: kvsend.at[f], kvrecv)
+    kvrecv[me_e] = kvsend[me_e]
 
     for i in (14, 15, 16):
         copies[i].wait()
-    def pass_on(g, p):
-        for r in range(half):
-            xt[r : r + 1, :] = ibox[g * half + r, :, 0:128]
-            xt[half + r : half + r + 1, :] = ibox[g * half + r, :, 128:256]
-        xg[g, my_k] = xt[...].astype(BF16)
-        put_tiles(p, xg.at[g])
-
-    arrived(10, ibox, half - 1)
-    pass_on(0, 7)
-    arrived(4, ibox, half)
-    pass_on(1, 11)
-
-    copies[3].wait()
-    copies[4].wait()
-    arrived(0, nrecv, ep_n - 1)
-    picked = nrecv[...].astype(F32).reshape(ep_n * seqs, 128).astype(BF16)
-    part = jnp.dot(picked, wpad[...], preferred_element_type=F32)
-    for f in range(ep_n):
-        kvsend[f, 0] = part[f * seqs : (f + 1) * seqs, :DH].astype(BF16)
-        kvsend[f, 1] = part[f * seqs : (f + 1) * seqs, DH:].astype(BF16)
-    put_ep(2, lambda f: kvsend.at[f], kvrecv)
-    kvrecv[me_e] = kvsend[me_e]
-
     lane = lax.broadcasted_iota(jnp.int32, (half, 128), 1)
 
     def expert(g, p, q):
@@ -637,6 +653,10 @@
         V((ep_n // 4 - 1, seqs, 128), BF16),
         V((2, seqs, DH), F32),
         V((2, seqs, DH), F32),
+        pltpu.SemaphoreType.REGULAR((tp_n // XN // 2 + 1,)),
+        pltpu.SemaphoreType.REGULAR((tp_n // XN // 2 + 1,)),
+        pltpu.SemaphoreType.REGULAR((2,)),
+        pltpu.SemaphoreType.REGULAR((2,)),
         pltpu.SemaphoreType.DMA((20,)),
         pltpu.SemaphoreType.DMA((13,)),
         pltpu.SemaphoreType.DMA((13,)),

time: 77.1 us -> 72.4 us (0.939)
  Pallas kernels: 75.7 us -> 70.9 us
    pallas_call x1, Pallas kernels: 75.1 us -> 70.3 us  [body(): pl.pallas_call(functools.partial(kernel, ep_n, tp_n), out_shape=tuple((V(...]
where the time goes in v3:
time: 72.4 us; the launch traced here: 72.2 us
  Pallas kernels  70.9 us (98%)
  between operations  1.29 us (2%)
    pallas_call x1, Pallas kernels, body(): pl.pallas_call(functools.partial(kernel, ep_n, tp_n), out_shape=tuple((V(...  70.3 us

profile of v3, /device:TPU:1, one launch (start us, length us, event | category | flops | bytes accessed | tf_op | source)
XLA Modules:
  0.0 72.2 jit_solution(162332154834227524)
XLA Ops:
  1.3 70.3 %decode_layer.1 = (bf16[8,64]{1,0:T(8,128)(2,1)S(1)}, bf16[8,128]{1,0:T(8,128)(2,1)S(1)}, bf16[8,128]{1,0:T(8,128)(2,1)S(1)}) custom-call(bf16[8,2048]{1,0:T(8,128)(2,1)} %tokens.1, f32[1,2048]{1,0:T(1,128)} %bitcast.14, bf16[64,128]{1,0:T(8,128)(2,1)} %wq.1, bf16[64,128]{1,0:T(8,128)(2,1)} %wk.1, bf16[64,128]{1,0:T(8,128)(2,1)} %wv.1, f32[1,128]{1,0:T(1,128)} %bitcast.19, ...), custom_call_target="tpu_custom_call" | custom-call | tf_op jit(solution)/shard_map/decode_layer/pallas_call | solution.py:667
  71.6 0.6 hand_over.1
